TPU v7x, 32 devices: a whole 2x2x4 slice. The times are simulated.
32 devices in a mesh: sp: 8 (over z, x), tp: 4 (over y, core).
Axes of the slice: x: 2, y: 2, z: 4, core: 2. Of those that a mesh axis runs over, the one named last changes fastest.
Arguments:
- residual: bfloat16 [6144, 2048], P('sp'), may hold values from -6 to 6
- query_matrix: bfloat16 [6144, 1024], P('sp', 'tp'), may hold values from -6 to 6
- key_matrix: bfloat16 [6144, 1024], P('sp', 'tp'), may hold values from -6 to 6
- value_matrix: bfloat16 [6144, 2048], P('sp', 'tp'), may hold values from -6 to 6
- output_gate_logit: bfloat16 [6144, 2048], P('sp', 'tp'), may hold values from -6 to 6
- input_gate_log: float32 [6144, 8], P('sp', 'tp'), may hold values from -4 to 125
- forget_gate_logit: float32 [6144, 8], P('sp', 'tp')
- extra_head_decay: float32 [6144, 8], P('sp', 'tp'), may hold values from -1 to 0
- head_norm_gain: float32 [2048], P('tp'), may hold values from 0.1 to 1.9
- projection: bfloat16 [2048, 2048], P('tp'), may hold values from -5.303301 to 5.303301
- cell_output_gain: float32 [2048], replicated, may hold values from 0.1 to 1.9
- mixer_input_gain: float32 [2048], replicated, may hold values from 0.1 to 1.9
- mixer_gate_weight: bfloat16 [2048, 5120], P('sp', 'tp'), may hold values from -0.125 to 0.125
- mixer_up_weight: bfloat16 [2048, 5120], P('sp', 'tp'), may hold values from -0.125 to 0.125
- mixer_down_weight: bfloat16 [5120, 2048], P('tp', 'sp'), may hold values from -0.078125 to 0.078125
Outputs:
- updated: bfloat16 [6144, 2048], P('sp', 'tp')
All inputs are finite; a program needn't handle non-finite values.
Results may differ from a plain program's by a relative error of at most 0.014.
Values may be sent and summed in bfloat16 or wider, within the bound.
A program may use at most 128 MiB of HBM per device.

v0:
```python
import jax
import jax.numpy as jnp
from jax import lax
from jax.sharding import PartitionSpec as P

DQK = 128
DV = 256
HIGHEST = lax.Precision.HIGHEST
EPSILON = 1e-06
LOWEST_LOG = -1e30


def carried_in(value, axis, join, neutral):
    count, mine = (lax.axis_size(axis), lax.axis_index(axis))
    pieces = jax.tree.map(lambda part: lax.all_gather(part, axis), value)
    subtotal = jax.tree.map(
        lambda part, zero: jnp.full_like(part, 0) + jnp.asarray(zero, part.dtype), value, neutral
    )

    def turn(position, subtotal):
        longer = join(subtotal, jax.tree.map(lambda part: part[position], pieces))
        return jax.tree.map(lambda new, old: jnp.where(position < mine, new, old), longer, subtotal)

    return lax.fori_loop(0, count - 1, turn, subtotal)


def heads_first(array, heads, width):
    return array.reshape(array.shape[0], heads, width).transpose(1, 0, 2)


def read_out(
    query_low, key_low, value_low, in_logs, running_log_total, memory, normalizer, stabilizer
):
    length = query_low.shape[1]
    causal = lax.broadcasted_iota(jnp.int32, (length, length), 0) >= lax.broadcasted_iota(
        jnp.int32, (length, length), 1
    )
    spread = running_log_total[:, :, None] - running_log_total[:, None, :] + in_logs[:, None, :]
    spread = jnp.where(causal[None], spread, -jnp.inf)
    carried = running_log_total + stabilizer[:, None]
    running = jnp.maximum(carried, jnp.max(spread, axis=-1))
    scores = jnp.einsum(
        "htd,hsd->hts", query_low, key_low, preferred_element_type=jnp.float32
    ) * DQK ** (-0.5)
    weights = jnp.exp(spread - running[:, :, None]) * scores
    scaled = jnp.exp(carried - running)
    scaled_query = query_low.astype(jnp.float32) * DQK ** (-0.5)
    numerator = jnp.einsum(
        "hts,hsv->htv", weights.astype(jnp.bfloat16), value_low, preferred_element_type=jnp.float32
    )
    numerator = numerator + scaled[:, :, None] * jnp.einsum(
        "hvd,htd->htv", memory, scaled_query, precision=HIGHEST
    )
    denominator = jnp.sum(weights, axis=-1) + scaled * jnp.einsum(
        "hd,htd->ht", normalizer, scaled_query, precision=HIGHEST
    )
    return numerator / jnp.maximum(jnp.abs(denominator), jnp.exp(-running))[:, :, None]


def fold_state(keyed, valued, in_logs, running_log_total, memory, normalizer, stabilizer):
    last = running_log_total[:, -1]
    lifted = last[:, None] - running_log_total + in_logs
    new_max = jnp.maximum(last + stabilizer, jnp.max(lifted, axis=-1))
    weights = jnp.exp(lifted - new_max[:, None])
    retained = jnp.exp(last + stabilizer - new_max)
    memory = retained[:, None, None] * memory + jnp.einsum(
        "hsv,hsd->hvd", weights[:, :, None] * valued, keyed, precision=HIGHEST
    )
    normalizer = retained[:, None] * normalizer + jnp.einsum(
        "hs,hsd->hd", weights, keyed, precision=HIGHEST
    )
    return (memory, normalizer, new_max)


def join_states(earlier, later):
    early_decay, early_memory, early_normalizer, early_max = earlier
    late_decay, late_memory, late_normalizer, late_max = later
    joined_max = jnp.maximum(late_decay + early_max, late_max)
    first_scale = jnp.exp(late_decay + early_max - joined_max)
    second_scale = jnp.exp(late_max - joined_max)
    memory = first_scale[:, None, None] * early_memory + second_scale[:, None, None] * late_memory
    normalizer = first_scale[:, None] * early_normalizer + second_scale[:, None] * late_normalizer
    return (early_decay + late_decay, memory, normalizer, joined_max)


def body(
    residual,
    query_matrix,
    key_matrix,
    value_matrix,
    output_gate_logit,
    input_gate_log,
    forget_gate_logit,
    extra_head_decay,
    head_norm_gain,
    projection,
    cell_output_gain,
    mixer_input_gain,
    mixer_gate_weight,
    mixer_up_weight,
    mixer_down_weight,
):
    tok_rows = residual.shape[0]
    width = residual.shape[1]
    heads_here = input_gate_log.shape[1]
    query_low = heads_first(query_matrix, heads_here, DQK)
    key_low = heads_first(key_matrix, heads_here, DQK)
    value_low = heads_first(value_matrix, heads_here, DV)
    keyed = key_low.astype(jnp.float32)
    valued = value_low.astype(jnp.float32)
    in_logs = input_gate_log.T
    running_log_total = jnp.cumsum(
        (jax.nn.log_sigmoid(forget_gate_logit) + extra_head_decay).T, axis=-1
    )
    zero_memory = jnp.zeros((heads_here, DV, DQK), jnp.float32)
    zero_normalizer = jnp.zeros((heads_here, DQK), jnp.float32)
    lowest = jnp.full((heads_here,), LOWEST_LOG, jnp.float32)
    local_memory, local_normalizer, local_max = fold_state(
        keyed, valued, in_logs, running_log_total, zero_memory, zero_normalizer, lowest
    )
    prior_decay, prior_memory, prior_normalizer, prior_max = carried_in(
        (running_log_total[:, -1], local_memory, local_normalizer, local_max),
        "sp",
        join_states,
        (jnp.zeros_like(lowest), zero_memory, zero_normalizer, lowest),
    )
    start_max = jnp.maximum(prior_decay, prior_max)
    lift = jnp.exp(prior_max - start_max)
    cells = read_out(
        query_low,
        key_low,
        value_low,
        in_logs,
        running_log_total,
        lift[:, None, None] * prior_memory,
        lift[:, None] * prior_normalizer,
        start_max,
    )
    centered = cells - jnp.mean(cells, axis=-1, keepdims=True)
    normed = centered * lax.rsqrt(jnp.mean(centered * centered, axis=-1, keepdims=True) + EPSILON)
    normed = normed * head_norm_gain.reshape(heads_here, DV)[:, None, :]
    normed = normed.transpose(1, 0, 2).reshape(tok_rows, heads_here * DV)
    gated = (normed * jax.nn.sigmoid(output_gate_logit.astype(jnp.float32))).astype(jnp.bfloat16)
    cols_here = width // lax.axis_size("tp")
    offset = lax.axis_index("tp") * cols_here
    columns = projection
    mixed = (
        lax.psum_scatter(
            lax.dot_general(
                columns, gated, (((0,), (1,)), ((), ())), preferred_element_type=jnp.float32
            ).astype(jnp.bfloat16),
            "tp",
            scatter_dimension=0,
            tiled=True,
        )
        .astype(jnp.float32)
        .T
    )
    squares = lax.psum(jnp.sum(mixed * mixed, axis=-1), "tp")
    mixed = (
        mixed
        * lax.rsqrt(squares / width + EPSILON)[:, None]
        * lax.dynamic_slice_in_dim(cell_output_gain, offset, cols_here, 0)
    )
    own_residual = lax.dynamic_slice_in_dim(residual, offset, cols_here, 1).astype(jnp.float32)
    first_sum = (own_residual + mixed).astype(jnp.bfloat16)
    own_first = lax.optimization_barrier(first_sum).astype(jnp.float32)
    first_total = lax.psum(jnp.sum(own_first * own_first, axis=-1), "tp")
    own_gain = lax.dynamic_slice_in_dim(mixer_input_gain, offset, cols_here, 0)
    normed_own = (own_first * lax.rsqrt(first_total / width + EPSILON)[:, None] * own_gain).astype(
        jnp.bfloat16
    )
    normed_rows = lax.all_gather(normed_own, "tp", axis=1, tiled=True)
    columns = normed_rows
    gate_value = jnp.dot(
        columns,
        lax.all_gather(mixer_gate_weight, "sp", axis=0, tiled=True),
        preferred_element_type=jnp.float32,
    )
    up_value = jnp.dot(
        columns,
        lax.all_gather(mixer_up_weight, "sp", axis=0, tiled=True),
        preferred_element_type=jnp.float32,
    )
    activated = (jax.nn.silu(gate_value) * up_value).astype(jnp.bfloat16)
    down_terms = jnp.dot(
        activated,
        lax.all_gather(mixer_down_weight, "sp", axis=1, tiled=True),
        preferred_element_type=jnp.float32,
    )
    channel_out = lax.psum_scatter(
        down_terms.astype(jnp.bfloat16), "tp", scatter_dimension=1, tiled=True
    ).astype(jnp.float32)
    return (own_first + 0.5 * channel_out).astype(jnp.bfloat16)


def solution(mesh):
    return jax.shard_map(
        body,
        mesh=mesh,
        in_specs=(
            P("sp", None),
            P("sp", "tp"),
            P("sp", "tp"),
            P("sp", "tp"),
            P("sp", "tp"),
            P("sp", "tp"),
            P("sp", "tp"),
            P("sp", "tp"),
            P("tp"),
            P("tp", None),
            P(),
            P(),
            P("sp", "tp"),
            P("sp", "tp"),
            P("tp", "sp"),
        ),
        out_specs=P("sp", "tp"),
        check_vma=False,
    )
```

profile of v0, /device:TPU:0, one launch (start us, length us, event | category | flops | bytes accessed | tf_op | source)
XLA Modules:
  0.0 489.8 jit_solution(3324282672585852311)
XLA Ops:
  6.6 0.9 fusion.53
  7.5 0.6 reduce-window.6
  8.7 0.9 fusion.71
  9.9 1.4 copy.54
  11.4 2.8 fusion.32
  14.4 0.6 dynamic-slice
  15.5 0.2 dynamic-update-slice
  15.8 22.4 %all-gather.3 = f32[8,1,2]{2,1,0:T(1,128)S(1)} all-gather(f32[1,1,2]{2,1,0:T(1,128)S(1)} %fusion.59), channel_id=1, replica_groups=mesh['sp'=8,'tp'=4] {'sp'}, dimensions={0}, use_global_device_ids=true | all-gather | bytes 72 | tf_op jit(solution)/shard_map/all_gather | solution.py:15
  38.1 17.6 %all-reduce = f32[16]{0:T(128)S(1)} all-reduce(f32[16]{0:T(128)S(1)} %dynamic-update-slice), channel_id=2, replica_groups=mesh['sp'=8,'tp'=4] {'sp'}, use_global_device_ids=true, to_apply=%add | all-reduce | flops 16 | bytes 128
  55.9 0.3 fusion.40
  56.2 18.9 %all-gather.4 = f32[8,2,128]{2,1,0:T(2,128)S(1)} all-gather(f32[1,2,128]{2,1,0:T(2,128)S(1)} %add_bitcast_fusion.1), channel_id=4, replica_groups=mesh['sp'=8,'tp'=4] {'sp'}, dimensions={0}, use_global_device_ids=true | all-gather | bytes 9216 | tf_op jit(solution)/shard_map/all_gather | solution.py:15
  75.4 0.9 fusion.7
  76.4 8.3 %while.20 = (s32[]{:T(128)}, f32[2]{0:T(128)S(1)}, f32[2,256,128]{2,1,0:T(8,128)S(1)}, f32[2,128]{1,0:T(2,128)S(1)}, f32[2]{0:T(128)S(1)}, /*index=5*/s32[]{:T(1...) while((s32[]{:T(128)}, f32[2]{0:T(128)S(1)}, ...), condition=%wide.region_4.5_spmd.clone, body=%wide.region_3.4_spmd.clone.sunk | while | flops 328984 | bytes 789781 | solution.py:24
  76.4 1.1 fusion.90
  77.6 1.1 fusion.90
  78.8 1.1 fusion.90
  80.0 1.1 fusion.90
  81.2 1.1 fusion.90
  82.4 1.1 fusion.90
  83.5 1.1 fusion.90
  84.8 3.0 fusion.10
  87.8 0.7 fusion.36
  88.5 1.5 fusion.37
  90.1 2.4 fusion.69
  92.5 0.3 multiply_reduce_fusion
  92.9 1.5 fusion.28
  94.4 3.1 copy.47
  97.5 4.9 fusion.9
  102.5 0.7 all-gather.13.cloned.1.call-update
  103.2 0.8 dynamic_slice.38
  104.0 0.8 dynamic_slice.39
  104.7 32.8 %reduce-scatter.3.cloned.1.call-done = bf16[512,768]{0,1:T(8,128)(2,1)} async-done(((bf16[2048,768]{0,1:T(8,128)(2,1)}), bf16[512,768]{0,1:T(8,128)(2,1)}) %reduce-scatter.3.cloned.1.call-update) | async-done | bytes 786448 | tf_op jit(solution)/shard_map/reduce_scatter | solution.py:148
  137.6 1.4 fusion.15
  138.9 5.8 %psum.14 = f32[768]{0:T(1024)S(1)} all-reduce(f32[768]{0:T(1024)S(1)} %fusion.15), channel_id=1, replica_groups=mesh['sp'=8,'tp'=4] {'tp'}, use_global_device_ids=true, to_apply=%region_11.12 | all-reduce | flops 768 | bytes 6144 | tf_op jit(solution)/shard_map/psum | solution.py:159
  144.7 1.7 fusion.19
  146.7 5.7 %psum.15 = f32[768]{0:T(1024)S(1)} all-reduce(f32[768]{0:T(1024)S(1)} %fusion.20), channel_id=1, replica_groups=mesh['sp'=8,'tp'=4] {'tp'}, use_global_device_ids=true, to_apply=%region_13.14 | all-reduce | flops 768 | bytes 6144 | tf_op jit(solution)/shard_map/psum | solution.py:168
  152.3 1.1 fusion.22
  153.5 0.5 all-gather.15.cloned.1.call-update
  154.1 0.5 all-gather.17.cloned.1.call-update
  154.7 0.3 reduce-scatter.5.cloned.1.call-start
  154.9 70.8 %all-gather.13.cloned.1.call-done = bf16[2048,1280]{1,0:T(8,128)(2,1)} async-done(((bf16[256,1280]{1,0:T(8,128)(2,1)}), bf16[2048,1280]{1,0:T(8,128)(2,1)}) %all-gather.13.cloned.1.call-update) | async-done | bytes 5242896 | tf_op jit(solution)/shard_map/all_gather | solution.py:177
  225.7 28.1 %all-gather.11.cloned.1.call-done = bf16[768,2048]{1,0:T(8,128)(2,1)} async-done(((bf16[768,512]{1,0:T(8,128)(2,1)}), bf16[768,2048]{1,0:T(8,128)(2,1)}) %all-gather.11.cloned.1.call-update) | async-done | bytes 3145744 | tf_op jit(solution)/shard_map/all_gather | solution.py:173
  253.8 9.6 %fusion.72 = f32[768,1280]{1,0:T(8,128)} fusion(bf16[768,2048]{1,0:T(8,128)(2,1)} %all-gather.11.cloned.1.call-done, bf16[2048,1280]{1,0:T(8,128)(2,1)} %all-gather.13.cloned.1.call-done), kind=kOutput, calls=%fused_computation.118 | convolution fusion | flops 4026531840 | bytes 12320768 | tf_op jit(solution)/shard_map/dot_general | solution.py:175
  263.4 78.4 %all-gather.15.cloned.1.call-done = bf16[2048,1280]{1,0:T(8,128)(2,1)} async-done(((bf16[256,1280]{1,0:T(8,128)(2,1)}), bf16[2048,1280]{1,0:T(8,128)(2,1)}) %all-gather.15.cloned.1.call-update) | async-done | bytes 5242896 | tf_op jit(solution)/shard_map/all_gather | solution.py:182
  341.8 86.9 %all-gather.17.cloned.1.call-done = bf16[1280,2048]{1,0:T(8,128)(2,1)} async-done(((bf16[1280,256]{1,0:T(8,128)(2,1)}), bf16[1280,2048]{1,0:T(8,128)(2,1)}) %all-gather.17.cloned.1.call-update) | async-done | bytes 5242896 | tf_op jit(solution)/shard_map/all_gather | solution.py:188
  428.7 16.0 %convolution_convert_fusion.1 = bf16[768,2048]{1,0:T(8,128)(2,1)} fusion(bf16[1280,2048]{1,0:T(8,128)(2,1)} %all-gather.17.cloned.1.call-done, bf16[768,2048]{1,0:T(8,128)(2,1)} %all-gather.11.cloned.1.call-done, bf16[2048,1280]{1,0:T(8,128)(2,1)} %all-gather.15.cloned.1.call-done, f32[768,1280]{1,0:T(8,128)} %fusion.72), kind=kOutput, calls=%fused_computation.23 | convolution fusion | flops 8060534784 | bytes 20709376 | tf_op jit(solution)/shard_map/dot_general | solution.py:186
  444.7 36.1 %reduce-scatter.5.cloned.1.call-done = bf16[768,512]{1,0:T(8,128)(2,1)} async-done(((bf16[768,2048]{1,0:T(8,128)(2,1)}), bf16[768,512]{1,0:T(8,128)(2,1)}) %reduce-scatter.5.cloned.1.call-update) | async-done | bytes 786448 | tf_op jit(solution)/shard_map/reduce_scatter | solution.py:191
  480.7 2.2 fusion.23
  (80 shorter events, 3.1 us)
Async XLA Ops:
  6.5 91.0 %copy-start = (bf16[512,2048]{1,0:T(8,128)(2,1)S(1)}, bf16[512,2048]{1,0:T(8,128)(2,1)}, u32[]{:S(2)}) copy-start(bf16[512,2048]{1,0:T(8,128)(2,1)} %param.26) | copy-start | bytes 6291460
  6.5 7.8 %copy-start.8 = (u32[32]{0:T(128)S(1)}, u32[32]{0:T(128)}, u32[]{:S(2)}) copy-start(u32[32]{0:T(128)} %constant.77) | copy-start | bytes 388
  6.5 49.4 %copy-start.4 = (bf16[768,256]{1,0:T(8,128)(2,1)S(1)}, bf16[768,256]{1,0:T(8,128)(2,1)}, u32[]{:S(2)}) copy-start(bf16[768,256]{1,0:T(8,128)(2,1)} %param.19) | copy-start | bytes 1179652
  6.5 49.3 %copy-start.6 = (f32[512]{0:T(512)S(1)}, f32[512]{0:T(512)}, u32[]{:S(2)}) copy-start(f32[512]{0:T(512)} %param.25) | copy-start | bytes 6148
  6.5 69.8 %all-gather.19.cloned.1.call-start = ((), (), s32[]{:S(2)}) async-start(), calls=%async_computation.8 | async-start | bytes 2359296 | tf_op jit(solution)/shard_map/all_gather | solution.py:15
  7.5 67.9 %copy-start.5 = (f32[768,2]{0,1:T(2,128)S(1)}, f32[768,2]{0,1:T(2,128)}, u32[]{:S(2)}) copy-start(f32[768,2]{0,1:T(2,128)} %param.22) | copy-start | bytes 18436
  11.3 26.8 %copy-start.1 = (bf16[768,512]{0,1:T(8,128)(2,1)}, bf16[768,512]{0,1:T(8,128)(2,1)S(1)}, u32[]{:S(2)}) copy-start(bf16[768,512]{0,1:T(8,128)(2,1)S(1)} %copy.54) | copy-start | bytes 2359300
  14.3 123.3 %reduce-scatter.3.cloned.1.call-start = ((), (), s32[]{:S(2)}) async-start(), calls=%async_computation.2 | async-start | bytes 3932160 | tf_op jit(solution)/shard_map/reduce_scatter | solution.py:148
  75.4 9.4 %copy-start.3 = (bf16[768,256]{1,0:T(8,128)(2,1)S(1)}, bf16[768,256]{1,0:T(8,128)(2,1)}, u32[]{:S(2)}) copy-start(bf16[768,256]{1,0:T(8,128)(2,1)} %param.18) | copy-start | bytes 1179652
  87.7 2.4 copy-start.2
  94.4 3.1 copy-start.7
  102.4 123.3 %all-gather.13.cloned.1.call-start = ((), (), s32[]{:S(2)}) async-start(), calls=%async_computation.4 | async-start | bytes 5898240 | tf_op jit(solution)/shard_map/all_gather | solution.py:177
  103.2 150.7 %all-gather.11.cloned.1.call-start = ((), (), s32[]{:S(2)}) async-start(), calls=%async_computation.3 | async-start | bytes 3932160 | tf_op jit(solution)/shard_map/all_gather | solution.py:173
  153.5 188.3 %all-gather.15.cloned.1.call-start = ((), (), s32[]{:S(2)}) async-start(), calls=%async_computation.5 | async-start | bytes 5898240 | tf_op jit(solution)/shard_map/all_gather | solution.py:182
  154.1 274.6 %all-gather.17.cloned.1.call-start = ((), (), s32[]{:S(2)}) async-start(), calls=%async_computation.6 | async-start | bytes 5898240 | tf_op jit(solution)/shard_map/all_gather | solution.py:188
  154.7 326.0 %reduce-scatter.5.cloned.1.call-start = ((), (), s32[]{:S(2)}) async-start(), calls=%async_computation.7 | async-start | bytes 3932160 | tf_op jit(solution)/shard_map/reduce_scatter | solution.py:191
Sparse Core Ops, SparseCore 0:
  14.4 52.0 all-gather.18
  102.5 34.9 reduce-scatter.2
  139.8 85.8 all-gather.12
  227.1 26.6 all-gather.10
  255.9 85.8 all-gather.14
  343.7 84.9 all-gather.16
  444.8 35.8 reduce-scatter.4
where the time goes:
time: 491 us; the launch traced here: 490 us
  waiting for transfers between devices  335 us (68%)
  blocking collectives  70.3 us (14%)
  matrix products  41 us (8%)
  other arithmetic  21.3 us (4%)
  between operations  14.3 us (3%)
  local copies, waits for them, and re-layouts  7.45 us (2%)
    all_gather x1, waiting for transfers between devices, body(): lax.all_gather(mixer_down_weight, 'sp', axis=1, tiled=True)  86.9 us
    all_gather x1, waiting for transfers between devices, body(): lax.all_gather(mixer_up_weight, 'sp', axis=0, tiled=True)  78.4 us
    all_gather x1, waiting for transfers between devices, body(): lax.all_gather(mixer_gate_weight, 'sp', axis=0, tiled=True)  70.8 us
    all_gather x2, blocking collectives, carried_in(): pieces = jax.tree.map(lambda part: lax.all_gather(part, axis), value)  41.3 us
    reduce_scatter x1, waiting for transfers between devices, body(): lax.psum_scatter(down_terms.astype(jnp.bfloat16), 'tp', scatter_dimension...  36.1 us
    reduce_scatter x1, waiting for transfers between devices, body(): lax.psum_scatter(lax.dot_general(columns, gated, (((0,), (1,)), ((), ()))...  32.8 us
    all_gather x1, waiting for transfers between devices, body(): normed_rows = lax.all_gather(normed_own, 'tp', axis=1, tiled=True)  28.1 us
    unnamed x1, blocking collectives  17.6 us
  transfers between devices with their start and end apart: 7, of which 6 were waited for; matrix products, arithmetic and copies ran while one was open for 4% of the time, Pallas kernels for 0%

commit v1 on v0

--- a/solution.py
+++ b/solution.py
@@ -2,6 +2,7 @@
 import jax.numpy as jnp
 from jax import lax
 from jax.sharding import PartitionSpec as P
+from jax.lax import all_gather
 
 DQK = 128
 DV = 256
@@ -183,11 +184,12 @@
         preferred_element_type=jnp.float32,
     )
     activated = (jax.nn.silu(gate_value) * up_value).astype(jnp.bfloat16)
-    down_terms = jnp.dot(
-        activated,
-        lax.all_gather(mixer_down_weight, "sp", axis=1, tiled=True),
-        preferred_element_type=jnp.float32,
-    )
+
+    def put_spot(local_block):
+        high = jnp.concatenate(all_gather(local_block, axis_name="sp"), axis=1)
+        return high
+
+    down_terms = jnp.dot(activated, put_spot(mixer_down_weight), preferred_element_type=jnp.float32)
     channel_out = lax.psum_scatter(
         down_terms.astype(jnp.bfloat16), "tp", scatter_dimension=1, tiled=True
     ).astype(jnp.float32)

time: 491 us -> 490 us (level)
  waiting for transfers between devices: 335 us -> 326 us
  local copies, waits for them, and re-layouts: 7.45 us -> 15.3 us
    all_gather x1, waiting for transfers between devices: 86.9 us -> 71.3 us  [put_spot(): high = jnp.concatenate(all_gather(local_block, axis_name='sp'), axis=1)]
    reshape x1 -> x2, local copies, waits for them, and re-layouts: 0.01 us -> 7.88 us  [the longest x1 7.87 us: put_spot(): high = jnp.concatenate(all_gather(local_block, axis_name='sp'), axis=1)]
    all_gather x1, waiting for transfers between devices: 70.8 us -> 78.3 us  [body(): lax.all_gather(mixer_gate_weight, 'sp', axis=0, tiled=True)]
  transfers between devices with their start and end apart: 7 -> 7, of which waited for: 6 -> 6; matrix products, arithmetic and copies ran while one was open for 4% -> 5% of each run, Pallas kernels for 0% -> 0%
where the time goes in v1:
time: 490 us; the launch traced here: 489 us
  waiting for transfers between devices  326 us (67%)
  blocking collectives  70.3 us (14%)
  matrix products  41.1 us (8%)
  other arithmetic  21.3 us (4%)
  local copies, waits for them, and re-layouts  15.3 us (3%)
  between operations  14.3 us (3%)
    all_gather x1, waiting for transfers between devices, body(): lax.all_gather(mixer_up_weight, 'sp', axis=0, tiled=True)  78.3 us
    all_gather x1, waiting for transfers between devices, body(): lax.all_gather(mixer_gate_weight, 'sp', axis=0, tiled=True)  78.3 us
    all_gather x1, waiting for transfers between devices, put_spot(): high = jnp.concatenate(all_gather(local_block, axis_name='sp'), axis=1)  71.3 us
    all_gather x2, blocking collectives, carried_in(): pieces = jax.tree.map(lambda part: lax.all_gather(part, axis), value)  41.3 us
    reduce_scatter x1, waiting for transfers between devices, body(): lax.psum_scatter(down_terms.astype(jnp.bfloat16), 'tp', scatter_dimension...  36.1 us
    reduce_scatter x1, waiting for transfers between devices, body(): lax.psum_scatter(lax.dot_general(columns, gated, (((0,), (1,)), ((), ()))...  32.3 us
    all_gather x1, waiting for transfers between devices, body(): normed_rows = lax.all_gather(normed_own, 'tp', axis=1, tiled=True)  28.1 us
    unnamed x1, blocking collectives  17.6 us
  transfers between devices with their start and end apart: 7, of which 6 were waited for; matrix products, arithmetic and copies ran while one was open for 5% of the time, Pallas kernels for 0%

profile of v1, /device:TPU:0, one launch (start us, length us, event | category | flops | bytes accessed | tf_op | source)
XLA Modules:
  0.0 489.0 jit_solution(18070727529678460058)
XLA Ops:
  6.6 0.9 fusion.53
  7.5 0.6 reduce-window.6
  8.7 0.9 fusion.71
  9.9 1.4 copy.56
  11.4 2.8 fusion.32
  14.4 0.6 dynamic-slice
  15.8 22.4 %all-gather.4 = f32[8,1,2]{2,1,0:T(1,128)S(1)} all-gather(f32[1,1,2]{2,1,0:T(1,128)S(1)} %fusion.59), channel_id=1, replica_groups=mesh['sp'=8,'tp'=4] {'sp'}, dimensions={0}, use_global_device_ids=true | all-gather | bytes 72 | tf_op jit(solution)/shard_map/all_gather | solution.py:16
  38.1 17.6 %all-reduce = f32[16]{0:T(128)S(1)} all-reduce(f32[16]{0:T(128)S(1)} %dynamic-update-slice), channel_id=2, replica_groups=mesh['sp'=8,'tp'=4] {'sp'}, use_global_device_ids=true, to_apply=%add | all-reduce | flops 16 | bytes 128
  55.9 0.3 fusion.40
  56.2 18.9 %all-gather.5 = f32[8,2,128]{2,1,0:T(2,128)S(1)} all-gather(f32[1,2,128]{2,1,0:T(2,128)S(1)} %add_bitcast_fusion.1), channel_id=4, replica_groups=mesh['sp'=8,'tp'=4] {'sp'}, dimensions={0}, use_global_device_ids=true | all-gather | bytes 9216 | tf_op jit(solution)/shard_map/all_gather | solution.py:16
  75.4 0.9 fusion.7
  76.4 8.3 %while.20 = (s32[]{:T(128)}, f32[2]{0:T(128)S(1)}, f32[2,256,128]{2,1,0:T(8,128)S(1)}, f32[2,128]{1,0:T(2,128)S(1)}, f32[2]{0:T(128)S(1)}, /*index=5*/s32[]{:T(1...) while((s32[]{:T(128)}, f32[2]{0:T(128)S(1)}, ...), condition=%wide.region_4.5_spmd.clone, body=%wide.region_3.4_spmd.clone.sunk | while | flops 328984 | bytes 789781 | solution.py:25
  76.4 1.1 fusion.90
  77.6 1.1 fusion.90
  78.8 1.1 fusion.90
  80.0 1.1 fusion.90
  81.2 1.1 fusion.90
  82.4 1.1 fusion.90
  83.5 1.1 fusion.90
  84.8 3.0 fusion.10
  87.8 0.7 fusion.36
  88.5 1.5 fusion.37
  90.1 2.4 fusion.69
  92.5 0.3 multiply_reduce_fusion
  92.9 1.5 fusion.28
  94.4 3.1 copy.48
  97.5 4.9 fusion.9
  102.5 0.7 all-gather.20.cloned.1.call-update
  103.2 0.5 all-gather.14.cloned.1.call-update
  103.8 0.8 dynamic_slice.38
  104.6 0.8 dynamic_slice.39
  105.3 32.3 %reduce-scatter.3.cloned.1.call-done = bf16[512,768]{0,1:T(8,128)(2,1)} async-done(((bf16[2048,768]{0,1:T(8,128)(2,1)}), bf16[512,768]{0,1:T(8,128)(2,1)}) %reduce-scatter.3.cloned.1.call-update) | async-done | bytes 786448 | tf_op jit(solution)/shard_map/reduce_scatter | solution.py:149
  137.6 1.4 fusion.15
  138.9 5.8 %psum.14 = f32[768]{0:T(1024)S(1)} all-reduce(f32[768]{0:T(1024)S(1)} %fusion.15), channel_id=1, replica_groups=mesh['sp'=8,'tp'=4] {'tp'}, use_global_device_ids=true, to_apply=%region_11.12 | all-reduce | flops 768 | bytes 6144 | tf_op jit(solution)/shard_map/psum | solution.py:160
  144.7 1.7 fusion.19
  146.7 5.7 %psum.15 = f32[768]{0:T(1024)S(1)} all-reduce(f32[768]{0:T(1024)S(1)} %fusion.20), channel_id=1, replica_groups=mesh['sp'=8,'tp'=4] {'tp'}, use_global_device_ids=true, to_apply=%region_13.14 | all-reduce | flops 768 | bytes 6144 | tf_op jit(solution)/shard_map/psum | solution.py:169
  152.3 1.1 fusion.22
  153.5 0.5 all-gather.16.cloned.1.call-update
  154.1 0.3 reduce-scatter.5.cloned.1.call-start
  154.3 71.3 %all-gather.20.cloned.1.call-done = bf16[10240,256]{1,0:T(8,128)(2,1)} async-done(((bf16[1280,256]{1,0:T(8,128)(2,1)}), bf16[10240,256]{1,0:T(8,128)(2,1)}) %all-gather.20.cloned.1.call-update) | async-done | bytes 5242896 | tf_op jit(solution)/shard_map/all_gather | solution.py:189
  225.7 7.9 %copy.49 = bf16[1280,8,256]{0,2,1:T(8,128)(2,1)} copy(bf16[1280,8,256]{2,0,1:T(8,128)(2,1)} %bitcast.182) | data formatting | bytes 10485760 | tf_op jit(solution)/shard_map/reshape | solution.py:189
  233.6 78.3 %all-gather.14.cloned.1.call-done = bf16[2048,1280]{1,0:T(8,128)(2,1)} async-done(((bf16[256,1280]{1,0:T(8,128)(2,1)}), bf16[2048,1280]{1,0:T(8,128)(2,1)}) %all-gather.14.cloned.1.call-update) | async-done | bytes 5242896 | tf_op jit(solution)/shard_map/all_gather | solution.py:178
  311.8 28.1 %all-gather.12.cloned.1.call-done = bf16[768,2048]{1,0:T(8,128)(2,1)} async-done(((bf16[768,512]{1,0:T(8,128)(2,1)}), bf16[768,2048]{1,0:T(8,128)(2,1)}) %all-gather.12.cloned.1.call-update) | async-done | bytes 3145744 | tf_op jit(solution)/shard_map/all_gather | solution.py:174
  340.0 9.6 %fusion.72 = f32[768,1280]{1,0:T(8,128)} fusion(bf16[768,2048]{1,0:T(8,128)(2,1)} %all-gather.12.cloned.1.call-done, bf16[2048,1280]{1,0:T(8,128)(2,1)} %all-gather.14.cloned.1.call-done), kind=kOutput, calls=%fused_computation.118 | convolution fusion | flops 4026531840 | bytes 12320768 | tf_op jit(solution)/shard_map/dot_general | solution.py:176
  349.6 78.3 %all-gather.16.cloned.1.call-done = bf16[2048,1280]{1,0:T(8,128)(2,1)} async-done(((bf16[256,1280]{1,0:T(8,128)(2,1)}), bf16[2048,1280]{1,0:T(8,128)(2,1)}) %all-gather.16.cloned.1.call-update) | async-done | bytes 5242896 | tf_op jit(solution)/shard_map/all_gather | solution.py:183
  427.9 16.0 %convolution_convert_fusion.1 = bf16[768,2048]{1,0:T(8,128)(2,1)} fusion(bf16[1280,2048]{0,1:T(8,128)(2,1)} %bitcast.183, bf16[768,2048]{1,0:T(8,128)(2,1)} %all-gather.12.cloned.1.call-done, bf16[2048,1280]{1,0:T(8,128)(2,1)} %all-gather.16.cloned.1.call-done, f32[768,1280]{1,0:T(8,128)} %fusion.72), kind=kOutput, calls=%fused_computation.23 | convolution fusion | flops 8060534784 | bytes 20709376 | tf_op jit(solution)/shard_map/dot_general | solution.py:192
  443.9 36.1 %reduce-scatter.5.cloned.1.call-done = bf16[768,512]{1,0:T(8,128)(2,1)} async-done(((bf16[768,2048]{1,0:T(8,128)(2,1)}), bf16[768,512]{1,0:T(8,128)(2,1)}) %reduce-scatter.5.cloned.1.call-update) | async-done | bytes 786448 | tf_op jit(solution)/shard_map/reduce_scatter | solution.py:193
  480.0 2.2 fusion.23
  (81 shorter events, 3.4 us)
Async XLA Ops:
  6.5 91.0 %copy-start = (bf16[512,2048]{1,0:T(8,128)(2,1)S(1)}, bf16[512,2048]{1,0:T(8,128)(2,1)}, u32[]{:S(2)}) copy-start(bf16[512,2048]{1,0:T(8,128)(2,1)} %param.26) | copy-start | bytes 6291460
  6.5 7.8 %copy-start.8 = (u32[32]{0:T(128)S(1)}, u32[32]{0:T(128)}, u32[]{:S(2)}) copy-start(u32[32]{0:T(128)} %constant.77) | copy-start | bytes 388
  6.5 49.4 %copy-start.4 = (bf16[768,256]{1,0:T(8,128)(2,1)S(1)}, bf16[768,256]{1,0:T(8,128)(2,1)}, u32[]{:S(2)}) copy-start(bf16[768,256]{1,0:T(8,128)(2,1)} %param.19) | copy-start | bytes 1179652
  6.5 49.3 %copy-start.6 = (f32[512]{0:T(512)S(1)}, f32[512]{0:T(512)}, u32[]{:S(2)}) copy-start(f32[512]{0:T(512)} %param.25) | copy-start | bytes 6148
  6.5 69.8 %all-gather.18.cloned.1.call-start = ((), (), s32[]{:S(2)}) async-start(), calls=%async_computation.7 | async-start | bytes 2359296 | tf_op jit(solution)/shard_map/all_gather | solution.py:16
  7.5 67.9 %copy-start.5 = (f32[768,2]{0,1:T(2,128)S(1)}, f32[768,2]{0,1:T(2,128)}, u32[]{:S(2)}) copy-start(f32[768,2]{0,1:T(2,128)} %param.22) | copy-start | bytes 18436
  11.3 26.8 %copy-start.1 = (bf16[768,512]{0,1:T(8,128)(2,1)}, bf16[768,512]{0,1:T(8,128)(2,1)S(1)}, u32[]{:S(2)}) copy-start(bf16[768,512]{0,1:T(8,128)(2,1)S(1)} %copy.56) | copy-start | bytes 2359300
  14.3 123.3 %reduce-scatter.3.cloned.1.call-start = ((), (), s32[]{:S(2)}) async-start(), calls=%async_computation.2 | async-start | bytes 3932160 | tf_op jit(solution)/shard_map/reduce_scatter | solution.py:149
  75.4 9.4 %copy-start.3 = (bf16[768,256]{1,0:T(8,128)(2,1)S(1)}, bf16[768,256]{1,0:T(8,128)(2,1)}, u32[]{:S(2)}) copy-start(bf16[768,256]{1,0:T(8,128)(2,1)} %param.18) | copy-start | bytes 1179652
  87.7 2.4 copy-start.2
  94.4 3.1 copy-start.7
  102.4 123.3 %all-gather.20.cloned.1.call-start = ((), (), s32[]{:S(2)}) async-start(), calls=%async_computation.8 | async-start | bytes 5898240 | tf_op jit(solution)/shard_map/all_gather | solution.py:189
  103.2 208.7 %all-gather.14.cloned.1.call-start = ((), (), s32[]{:S(2)}) async-start(), calls=%async_computation.4 | async-start | bytes 5898240 | tf_op jit(solution)/shard_map/all_gather | solution.py:178
  103.7 236.2 %all-gather.12.cloned.1.call-start = ((), (), s32[]{:S(2)}) async-start(), calls=%async_computation.3 | async-start | bytes 3932160 | tf_op jit(solution)/shard_map/all_gather | solution.py:174
  153.5 274.4 %all-gather.16.cloned.1.call-start = ((), (), s32[]{:S(2)}) async-start(), calls=%async_computation.5 | async-start | bytes 5898240 | tf_op jit(solution)/shard_map/all_gather | solution.py:183
  154.1 325.9 %reduce-scatter.5.cloned.1.call-start = ((), (), s32[]{:S(2)}) async-start(), calls=%async_computation.6 | async-start | bytes 3932160 | tf_op jit(solution)/shard_map/reduce_scatter | solution.py:193
Sparse Core Ops, SparseCore 0:
  14.4 52.0 all-gather.17
  102.5 34.9 reduce-scatter.2
  139.8 85.8 all-gather.19
  227.7 84.0 all-gather.13
  313.2 26.6 all-gather.11
  342.0 85.8 all-gather.15
  444.0 35.8 reduce-scatter.4
